TPU v7x, 32 devices: a whole 2x2x4 slice. The times are simulated.
32 devices in a mesh: ep: 4 (over y, x), tp: 8 (over z, core).
Axes of the slice: x: 2, y: 2, z: 4, core: 2. Of those that a mesh axis runs over, the one named last changes fastest.
Arguments:
- pool_input: bfloat16 [4096, 1024], P('ep', 'tp'), may hold values from -6 to 6
- pool_gain: float32 [1024], P('tp'), may hold values from 0.1 to 1.9
- mix_weight: bfloat16 [1024, 2048], P('tp'), may hold values from -0.1875 to 0.1875
- moe_input: bfloat16 [8192, 2048], P(('ep', 'tp')), may hold values from -6 to 6
- moe_gain: float32 [2048], replicated, may hold values from 0.1 to 1.9
- expert_ids: int32 [8192, 2], P(('ep', 'tp')), may hold values from 0 to 15, as said below
- route_weight: float32 [8192, 2], P(('ep', 'tp')), may hold values from 0.2 to 1
- gate_weight: bfloat16 [16, 2048, 1024], P('ep', None, 'tp'), may hold values from -0.125 to 0.125
- up_weight: bfloat16 [16, 2048, 1024], P('ep', None, 'tp'), may hold values from -0.125 to 0.125
- down_weight: bfloat16 [16, 2048, 1024], P('ep', None, 'tp'), may hold values from -0.1875 to 0.1875
Outputs:
- mixed_out: bfloat16 [4096, 2048], P(('ep', 'tp'))
- moe_out: bfloat16 [8192, 2048], P(('ep', 'tp'))
Inputs may be any that keep to these rules, and one draw needn't show every extreme that they name: `expert_ids`: each row names 2 different experts of one group of 4 consecutive experts. In each aligned block of 256 rows (the rows of one device) no expert is named by more than 48 rows, and some expert is named by exactly 48 rows.
All inputs are finite; a program needn't handle non-finite values.
Results may differ from a plain program's by a relative error of at most 0.012.
Values may be sent and summed in bfloat16 or wider, within the bound.
A program may use at most 128 MiB of HBM per device.

v0:
```python
import jax
import jax.numpy as jnp
from jax import lax
from jax.sharding import PartitionSpec as P

GROUP_CH = 256
EXPERTS = 16
GROUP_EXP = 4
TOP = 2
CAP = 48
CHUNKS = 2
eps_norm = 1e-06


def from_behind(shard, axis, by):
    peers = lax.axis_size(axis)
    pairs = [(i, i + by) for i in range(peers) if 0 <= i + by < peers]
    return lax.ppermute(shard, axis, pairs)


def window_sums(extended, row_count):
    level_sum = extended
    stride = 1
    outputs = []
    for doubling in range(4):
        level_sum = level_sum[stride:] + level_sum[:-stride]
        stride = stride * 2
        outputs.append(level_sum[level_sum.shape[0] - row_count :])
    return outputs


def pool_mixer(pool_input, pool_gain):
    row_count, channels = pool_input.shape
    carried = from_behind(pool_input[row_count - 15 :], "ep", 1)
    extended = jnp.concatenate([carried, pool_input], axis=0).astype(jnp.float32)
    window_list = window_sums(extended, row_count)
    channel_ids = lax.axis_index("tp") * channels + lax.iota(jnp.int32, channels)
    group_ids = channel_ids // GROUP_CH
    position = lax.axis_index("ep") * row_count + lax.iota(jnp.int32, row_count)
    summed = jnp.zeros((row_count, channels), jnp.float32)
    widths = jnp.zeros((channels,), jnp.int32)
    for index_group in range(4):
        inside = group_ids == index_group
        summed = jnp.where(inside[None, :], window_list[index_group], summed)
        widths = jnp.where(inside, 2 ** (index_group + 1), widths)
    counted = jnp.minimum(position[:, None] + 1, widths[None, :]).astype(jnp.float32)
    values = extended[15:]
    return ((summed / counted - values) * pool_gain).astype(jnp.bfloat16)


def dispatch_plan(expert_ids, route_weight, ep_size):
    local_experts = EXPERTS // ep_size
    share = TOP if local_experts % GROUP_EXP == 0 else 1
    capacity = local_experts * CAP // share
    owners = expert_ids // local_experts
    ep_index = lax.iota(jnp.int32, ep_size)
    member = jnp.any(owners[:, :, None] == ep_index[None, None, :], axis=1)
    counts = member.astype(jnp.int32)
    rank = jnp.cumsum(counts, axis=0) - counts
    slot = jnp.where(member, rank, -1).T
    placing = slot[:, None, :] == lax.iota(jnp.int32, capacity)[None, :, None]
    dense_weight = jnp.sum(
        jnp.where(
            expert_ids[:, :, None] == lax.iota(jnp.int32, EXPERTS)[None, None, :],
            route_weight[:, :, None],
            0.0,
        ),
        axis=1,
    )
    dense_weight = dense_weight.reshape(-1, ep_size, local_experts)
    slot_weight = jnp.einsum(
        "ecn,nej->ecj", placing.astype(jnp.float32), dense_weight, precision=lax.Precision.HIGHEST
    )
    return (placing.astype(jnp.bfloat16).reshape(ep_size * capacity, -1), slot_weight, capacity)


def body(
    pool_input,
    pool_gain,
    mix_weight,
    moe_input,
    moe_gain,
    expert_ids,
    route_weight,
    gate_weight,
    up_weight,
    down_weight,
):
    pooled = pool_mixer(pool_input, pool_gain)
    ep_size = lax.axis_size("ep")
    out_columns = mix_weight.shape[1] // ep_size
    mix_columns = lax.dynamic_slice_in_dim(
        mix_weight, lax.axis_index("ep") * out_columns, out_columns, axis=1
    )
    mix_columns = lax.all_gather(mix_columns, "tp", axis=0, tiled=True)
    inputs = moe_input.astype(jnp.float32)
    scale_rows = lax.rsqrt(jnp.mean(inputs * inputs, axis=-1, keepdims=True) + eps_norm)
    normed = (inputs * scale_rows * moe_gain).astype(jnp.bfloat16)
    placing, slot_weight, capacity = dispatch_plan(expert_ids, route_weight, ep_size)
    rows = capacity // CHUNKS
    arrived_list = []
    placing_list = []
    for chunk in range(CHUNKS):
        chunk_placing = placing.reshape(ep_size, capacity, -1)[:, chunk * rows : (chunk + 1) * rows]
        chunk_placing = chunk_placing.reshape(ep_size * rows, -1)
        outgoing = jnp.dot(chunk_placing, normed, preferred_element_type=jnp.float32)
        outgoing = outgoing.astype(jnp.bfloat16)
        placing_list.append(chunk_placing)
        arrived_list.append(lax.all_to_all(outgoing, "ep", split_axis=0, concat_axis=0, tiled=True))
    arrived_list[0], mix_columns = lax.optimization_barrier((arrived_list[0], mix_columns))
    weights = lax.all_to_all(slot_weight, "ep", split_axis=0, concat_axis=0, tiled=True)
    weights = lax.all_gather(weights, "tp", axis=0, tiled=True)
    combined = jnp.zeros(normed.shape, jnp.float32)
    for chunk in range(CHUNKS):
        tokens = lax.all_gather(arrived_list[chunk], "tp", axis=0, tiled=True)
        scales = weights[:, chunk * rows : (chunk + 1) * rows].reshape(tokens.shape[0], -1)
        gate_part = jnp.einsum(
            "nd,edf->enf", tokens, gate_weight, preferred_element_type=jnp.float32
        )
        upward = jnp.einsum("nd,edf->enf", tokens, up_weight, preferred_element_type=jnp.float32)
        hidden = (jax.nn.silu(gate_part) * upward * scales.T[:, :, None]).astype(jnp.bfloat16)
        partial = jnp.einsum("enf,edf->nd", hidden, down_weight, preferred_element_type=jnp.float32)
        reduced = lax.psum_scatter(
            partial.astype(jnp.bfloat16), "tp", scatter_dimension=0, tiled=True
        )
        returned = lax.all_to_all(reduced, "ep", split_axis=0, concat_axis=0, tiled=True)
        combined = combined + lax.dot_general(
            placing_list[chunk],
            returned,
            (((0,), (0,)), ((), ())),
            preferred_element_type=jnp.float32,
        )
    moe_out = combined.astype(jnp.bfloat16)
    regrouped = lax.all_to_all(pooled, "tp", split_axis=0, concat_axis=1, tiled=True)
    half = regrouped.shape[1] // 2
    mixed_sum = 0.0
    for part in range(2):
        section = slice(part * half, (part + 1) * half)
        pooled_rows = lax.all_gather(regrouped[:, section], "ep", axis=0, tiled=True)
        mixed_sum = mixed_sum + jnp.dot(
            pooled_rows, mix_columns[section], preferred_element_type=jnp.float32
        )
    mixed_out = lax.all_to_all(
        mixed_sum.astype(jnp.bfloat16), "ep", split_axis=0, concat_axis=1, tiled=True
    )
    return (mixed_out, moe_out)


def solution(mesh):
    return jax.shard_map(
        body,
        mesh=mesh,
        in_specs=(
            P("ep", "tp"),
            P("tp"),
            P("tp", None),
            P(("ep", "tp"), None),
            P(),
            P(("ep", "tp"), None),
            P(("ep", "tp"), None),
            P("ep", None, "tp"),
            P("ep", None, "tp"),
            P("ep", None, "tp"),
        ),
        out_specs=(P(("ep", "tp"), None), P(("ep", "tp"), None)),
        check_vma=False,
    )
```

profile of v0, /device:TPU:0, one launch (start us, length us, event | category | flops | bytes accessed | tf_op | source)
XLA Modules:
  0.0 334.8 jit_solution(6030024763773392144)
XLA Ops:
  7.3 1.7 constant_dynamic-slice_fusion
  9.1 0.7 and_select_fusion
  9.8 1.5 fusion.40
  11.3 1.2 reduce-window.6
  12.5 0.1 slice.101
  12.6 0.1 copy.45
  12.8 0.1 copy.46
  12.8 0.1 add_bitcast_fusion
  12.9 0.1 iota_compare_fusion
  13.0 1.7 convolution_convert_fusion
  14.8 16.4 %all_to_all.85 = bf16[4,48,2048]{2,1,0:T(8,128)(2,1)} all-to-all(bf16[4,48,2048]{2,1,0:T(8,128)(2,1)S(1)} %bitcast.128), channel_id=1, replica_groups=mesh['ep'=4,'tp'=8] {'ep'}, dimensions={0} | all-to-all | bytes 1572864 | tf_op jit(solution)/shard_map/all_to_all | solution.py:109
  31.3 0.5 convolution_convert_fusion.1
  31.8 13.2 %all_to_all.86 = bf16[4,48,2048]{2,1,0:T(8,128)(2,1)} all-to-all(bf16[4,48,2048]{2,1,0:T(8,128)(2,1)S(1)} %bitcast.127), channel_id=1, replica_groups=mesh['ep'=4,'tp'=8] {'ep'}, dimensions={0} | all-to-all | bytes 1572864 | tf_op jit(solution)/shard_map/all_to_all | solution.py:109
  45.2 0.3 fusion.65
  45.4 7.0 %all_to_all.87 = f32[4,96,4]{1,2,0:T(4,128)S(1)} all-to-all(f32[4,96,4]{1,2,0:T(4,128)S(1)} %fusion.65), channel_id=1, replica_groups=mesh['ep'=4,'tp'=8] {'ep'}, dimensions={0} | all-to-all | bytes 12288 | tf_op jit(solution)/shard_map/all_to_all | solution.py:111
  52.5 14.8 %all_gather.22 = f32[32,96,4]{1,2,0:T(4,128)S(1)} all-gather(f32[4,96,4]{1,2,0:T(4,128)S(1)} %all_to_all.87), channel_id=1, replica_groups=mesh['ep'=4,'tp'=8] {'tp'}, dimensions={0}, use_global_device_ids=true | all-gather | bytes 55296 | tf_op jit(solution)/shard_map/all_gather | solution.py:112
  67.3 0.1 fusion.72
  67.4 0.1 reshape.106
  67.5 34.2 %all-gather.8.cloned.1.call-done = bf16[1536,2048]{1,0:T(8,128)(2,1)} async-done(((bf16[192,2048]{1,0:T(8,128)(2,1)}), bf16[1536,2048]{1,0:T(8,128)(2,1)}) %all-gather.8.cloned.1.call-update) | async-done | bytes 6291472 | tf_op jit(solution)/shard_map/all_gather | solution.py:115
  101.7 8.5 %fusion.20 = f32[4,1536,128]{2,1,0:T(8,128)} fusion(bf16[4,2048,128]{2,1,0:T(8,128)(2,1)} %param.17, bf16[1536,2048]{1,0:T(8,128)(2,1)} %all-gather.8.cloned.1.call-done), kind=kOutput, calls=%fused_computation.14 | convolution fusion | flops 3221225472 | bytes 11534336 | tf_op jit(solution)/shard_map/nd,edf->enf/dot_general | solution.py:117
  110.2 12.3 %bitcast_convert_fusion = bf16[1536,2048]{1,0:T(8,128)(2,1)} fusion(bf16[4,2048,128]{2,1,0:T(8,128)(2,1)S(1)} %copy-done, bf16[4,2048,128]{2,1,0:T(8,128)(2,1)} %param.18, bf16[1536,2048]{1,0:T(8,128)(2,1)} %all-gather.8.cloned.1.call-done, f32[4,1536,128]{2,1,0:T(8,128)} %fusion.20, f32[4,1536]{1,0:T(4,128)S(1)} %bitcast.132), kind=kOutput, calls=%fused_computation | convolution fusion | flops 6451101696 | bytes 19947520 | tf_op jit(solution)/shard_map/enf,edf->nd/dot_general | solution.py:122
  122.5 0.2 reduce-scatter.3.cloned.1.call-start
  122.8 0.1 reshape.104
  122.9 43.8 %all-gather.6.cloned.1.call-done = bf16[1536,2048]{1,0:T(8,128)(2,1)} async-done(((bf16[192,2048]{1,0:T(8,128)(2,1)}), bf16[1536,2048]{1,0:T(8,128)(2,1)}) %all-gather.6.cloned.1.call-update) | async-done | bytes 6291472 | tf_op jit(solution)/shard_map/all_gather | solution.py:115
  166.7 8.5 %fusion.8 = f32[4,1536,128]{2,1,0:T(8,128)} fusion(bf16[4,2048,128]{2,1,0:T(8,128)(2,1)} %param.17, bf16[1536,2048]{1,0:T(8,128)(2,1)} %all-gather.6.cloned.1.call-done), kind=kOutput, calls=%fused_computation.10 | convolution fusion | flops 3221225472 | bytes 11534336 | tf_op jit(solution)/shard_map/nd,edf->enf/dot_general | solution.py:117
  175.3 11.8 %bitcast_convert_fusion.1 = bf16[1536,2048]{1,0:T(8,128)(2,1)} fusion(bf16[4,2048,128]{2,1,0:T(8,128)(2,1)S(1)} %copy-done, bf16[4,2048,128]{2,1,0:T(8,128)(2,1)} %param.18, bf16[1536,2048]{1,0:T(8,128)(2,1)} %all-gather.6.cloned.1.call-done, f32[4,1536,128]{2,1,0:T(8,128)} %fusion.8, f32[4,1536]{1,0:T(4,128)S(1)} %bitcast.133), kind=kOutput, calls=%fused_computation.1 | convolution fusion | flops 6451101696 | bytes 19947520 | tf_op jit(solution)/shard_map/enf,edf->nd/dot_general | solution.py:122
  187.1 0.9 copy-done.3
  188.0 3.5 %collective-permute-start = (bf16[15,128]{1,0:T(8,128)(2,1)S(1)}, bf16[15,128]{1,0:T(8,128)(2,1)S(1)}, u32[]{:S(2)}, u32[]{:S(2)}) collective-permute-start(bf16[15,128]{1,0:T(8,128)(2,1)S(1)} %slice.67), channel_id=1, source_target_pairs={{0,8},{8,16},{16,24},{1,9},{9,17},{17,25},{2,10},{10,18},{18,26},{... | collective-permute-start | bytes 11528 | tf_op jit(solution)/shard_map/ppermute | solution.py:18
  191.6 1.2 collective-permute-done
  192.8 0.1 maximum_convert_fusion
  192.9 0.1 slice_add_fusion.1
  193.0 0.1 slice_add_fusion
  193.0 0.1 slice_add_fusion.2
  193.1 0.4 fusion.53
  193.5 17.3 %all_to_all.88 = bf16[8,128,128]{2,1,0:T(8,128)(2,1)} all-to-all(bf16[8,128,128]{2,1,0:T(8,128)(2,1)S(1)} %bitcast.122), channel_id=1, replica_groups=mesh['ep'=4,'tp'=8] {'tp'}, dimensions={0} | all-to-all | bytes 524288 | tf_op jit(solution)/shard_map/all_to_all | solution.py:134
  210.8 1.1 copy.44
  212.0 11.7 %all_gather.18 = bf16[512,512]{0,1:T(8,128)(2,1)S(1)} all-gather(bf16[128,512]{0,1:T(8,128)(2,1)S(1)} %get-tuple-element.7), channel_id=1, replica_groups=mesh['ep'=4,'tp'=8] {'ep'}, dimensions={0}, use_global_device_ids=true | all-gather | bytes 655360 | tf_op jit(solution)/shard_map/all_gather | solution.py:139
  223.7 9.1 %all_gather.20 = bf16[512,512]{0,1:T(8,128)(2,1)S(1)} all-gather(bf16[128,512]{0,1:T(8,128)(2,1)S(1)} %get-tuple-element.6), channel_id=1, replica_groups=mesh['ep'=4,'tp'=8] {'ep'}, dimensions={0}, use_global_device_ids=true | all-gather | bytes 655360 | tf_op jit(solution)/shard_map/all_gather | solution.py:139
  232.8 0.5 fusion.59
  233.2 0.5 fusion.51
  233.7 10.3 %all_to_all.89 = bf16[4,128,512]{2,1,0:T(8,128)(2,1)S(1)} all-to-all(bf16[4,128,512]{2,1,0:T(8,128)(2,1)S(1)} %bitcast.120), channel_id=1, replica_groups=mesh['ep'=4,'tp'=8] {'ep'}, dimensions={0} | all-to-all | bytes 1048576 | tf_op jit(solution)/shard_map/all_to_all | solution.py:143
  244.0 12.8 %all_to_all.90 = bf16[4,48,2048]{2,1,0:T(8,128)(2,1)} all-to-all(bf16[4,48,2048]{2,1,0:T(8,128)(2,1)} %bitcast.125), channel_id=1, replica_groups=mesh['ep'=4,'tp'=8] {'ep'}, dimensions={0} | all-to-all | bytes 1572864 | tf_op jit(solution)/shard_map/all_to_all | solution.py:126
  256.9 55.6 %reduce-scatter.3.cloned.1.call-done = bf16[192,2048]{1,0:T(8,128)(2,1)} async-done(((bf16[1536,2048]{1,0:T(8,128)(2,1)}), bf16[192,2048]{1,0:T(8,128)(2,1)}) %reduce-scatter.3.cloned.1.call-update) | async-done | bytes 786448 | tf_op jit(solution)/shard_map/reduce_scatter | solution.py:123
  312.5 3.6 %all-to-all-start.4 = ((bf16[4,48,2048]{2,1,0:T(8,128)(2,1)}), bf16[4,48,2048]{2,1,0:T(8,128)(2,1)S(1)}, u32[]{:S(2)}, u32[]{:S(2)}) async-start(bf16[4,48,2048]{2,1,0:T(8,128)(2,1)} %bitcast.126), calls=%async_computation.5 | async-start | bytes 1572864 | tf_op jit(solution)/shard_map/all_to_all | solution.py:126
  316.1 0.8 copy.50
  317.0 3.0 convolution_bitcast_fusion
  319.9 5.3 %all-to-all-done.4 = bf16[4,48,2048]{2,1,0:T(8,128)(2,1)S(1)} async-done(((bf16[4,48,2048]{2,1,0:T(8,128)(2,1)}), bf16[4,48,2048]{2,1,0:T(8,128)(2,1)S(1)}, u32[]{:S(2)}, u32[]{:S(2)}) %all-to-all-start.4) | async-done | bytes 786464 | tf_op jit(solution)/shard_map/all_to_all | solution.py:126
  325.2 3.1 fusion.39
  (44 shorter events, 0.5 us)
Async XLA Ops:
  7.2 103.1 %copy-start = (bf16[4,2048,128]{2,1,0:T(8,128)(2,1)S(1)}, bf16[4,2048,128]{2,1,0:T(8,128)(2,1)}, u32[]{:S(2)}) copy-start(bf16[4,2048,128]{2,1,0:T(8,128)(2,1)} %param.19) | copy-start | bytes 6291460
  7.2 37.9 %all-gather.4.cloned.1.call-start = ((), (), s32[]{:S(2)}) async-start(), calls=%async_computation.9 | async-start | bytes 1179648 | tf_op jit(solution)/shard_map/all_gather | solution.py:95
  7.2 24.0 %copy-start.1 = (bf16[256,2048]{1,0:T(8,128)(2,1)S(1)}, bf16[256,2048]{1,0:T(8,128)(2,1)}, u32[]{:S(2)}) copy-start(bf16[256,2048]{1,0:T(8,128)(2,1)} %param.13) | copy-start | bytes 3145732
  7.2 24.0 %copy-start.7 = (f32[2048]{0:T(1024)S(1)}, f32[2048]{0:T(1024)}, u32[]{:S(2)}) copy-start(f32[2048]{0:T(1024)} %param.14) | copy-start | bytes 24580
  9.0 92.7 %all-gather.8.cloned.1.call-start = ((), (), s32[]{:S(2)}) async-start(), calls=%async_computation.12 | async-start | bytes 7077888 | tf_op jit(solution)/shard_map/all_gather | solution.py:115
  14.7 30.4 %copy-start.4 = (s32[256,2]{0,1:T(2,128)S(1)}, s32[256,2]{0,1:T(2,128)}, u32[]{:S(2)}) copy-start(s32[256,2]{0,1:T(2,128)} %param.15) | copy-start | bytes 6148
  14.8 30.4 %copy-start.5 = (f32[256,2]{0,1:T(2,128)S(1)}, f32[256,2]{0,1:T(2,128)}, u32[]{:S(2)}) copy-start(f32[256,2]{0,1:T(2,128)} %param.16) | copy-start | bytes 6148
  31.2 135.5 %all-gather.6.cloned.1.call-start = ((), (), s32[]{:S(2)}) async-start(), calls=%async_computation.10 | async-start | bytes 7077888 | tf_op jit(solution)/shard_map/all_gather | solution.py:115
  45.1 199.0 %reduce-scatter.5.cloned.1.call-start = ((), (), s32[]{:S(2)}) async-start(), calls=%async_computation.13 | async-start | bytes 7077888 | tf_op jit(solution)/shard_map/reduce_scatter | solution.py:123
  122.5 189.9 %reduce-scatter.3.cloned.1.call-start = ((), (), s32[]{:S(2)}) async-start(), calls=%async_computation.11 | async-start | bytes 7077888 | tf_op jit(solution)/shard_map/reduce_scatter | solution.py:123
  187.0 0.9 copy-start.3
  188.0 5.1 %copy-start.6 = (f32[128]{0:T(128)S(1)}, f32[128]{0:T(128)}, u32[]{:S(2)}) copy-start(f32[128]{0:T(128)} %param.11) | copy-start | bytes 1540
  188.0 4.8 %collective-permute-start = (bf16[15,128]{1,0:T(8,128)(2,1)S(1)}, bf16[15,128]{1,0:T(8,128)(2,1)S(1)}, u32[]{:S(2)}, u32[]{:S(2)}) collective-permute-start(bf16[15,128]{1,0:T(8,128)(2,1)S(1)} %slice.67), channel_id=1, source_target_pairs={{0,8},{8,16},{16,24},{1,9},{9,17},{17,25},{2,10},{10,18},{18,26},{... | collective-permute-start | bytes 11528 | tf_op jit(solution)/shard_map/ppermute | solution.py:18
  193.1 39.7 %copy-start.2 = (bf16[1024,512]{1,0:T(8,128)(2,1)S(1)}, bf16[1024,512]{1,0:T(8,128)(2,1)}, u32[]{:S(2)}) copy-start(bf16[1024,512]{1,0:T(8,128)(2,1)} %all-gather.4.cloned.1.call-done) | copy-start | bytes 3145732
  312.5 12.7 %all-to-all-start.4 = ((bf16[4,48,2048]{2,1,0:T(8,128)(2,1)}), bf16[4,48,2048]{2,1,0:T(8,128)(2,1)S(1)}, u32[]{:S(2)}, u32[]{:S(2)}) async-start(bf16[4,48,2048]{2,1,0:T(8,128)(2,1)} %bitcast.126), calls=%async_computation.5 | async-start | bytes 1572864 | tf_op jit(solution)/shard_map/all_to_all | solution.py:126
Sparse Core Ops, SparseCore 0:
  10.2 24.9 all-gather.3
  36.8 64.8 all-gather.7
  103.4 63.3 all-gather.5
  168.9 72.5 reduce-scatter.4
  243.7 68.7 reduce-scatter.2
where the time goes:
time: 336 us; the launch traced here: 335 us
  waiting for transfers between devices  140 us (42%)
  blocking collectives  113 us (34%)
  matrix products  50.6 us (15%)
  between operations  14 us (4%)
  starting transfers between devices  7.53 us (2%)
  local copies, waits for them, and re-layouts  5.31 us (2%)
  other arithmetic  4.27 us (1%)
    all_gather x2, waiting for transfers between devices, body(): tokens = lax.all_gather(arrived_list[chunk], 'tp', axis=0, tiled=True)  78 us
    reduce_scatter x2, waiting for transfers between devices, body(): lax.psum_scatter(partial.astype(jnp.bfloat16), 'tp', scatter_dimension=0,...  55.6 us
    all_to_all x2, blocking collectives, body(): lax.all_to_all(outgoing, 'ep', split_axis=0, concat_axis=0, tiled=True)  29.7 us
    dot_general x2, matrix products, body(): jnp.einsum('enf,edf->nd', hidden, down_weight, preferred_element_type=jnp...  24.1 us
    all_gather x2, blocking collectives, body(): lax.all_gather(regrouped[:, section], 'ep', axis=0, tiled=True)  20.8 us
    all_to_all x1, blocking collectives, body(): lax.all_to_all(pooled, 'tp', split_axis=0, concat_axis=1, tiled=True)  17.3 us
    dot_general x2, matrix products, body(): jnp.einsum('nd,edf->enf', tokens, gate_weight, preferred_element_type=jnp...  17 us
    all_gather x1, blocking collectives, body(): weights = lax.all_gather(weights, 'tp', axis=0, tiled=True)  14.8 us
  transfers between devices with their start and end apart: 7, of which 5 were waited for; matrix products, arithmetic and copies ran while one was open for 16% of the time, Pallas kernels for 0%

commit v1 on v0

--- a/solution.py
+++ b/solution.py
@@ -112,7 +112,14 @@
     weights = lax.all_gather(weights, "tp", axis=0, tiled=True)
     combined = jnp.zeros(normed.shape, jnp.float32)
     for chunk in range(CHUNKS):
-        tokens = lax.all_gather(arrived_list[chunk], "tp", axis=0, tiled=True)
+        ring = [arrived_list[chunk]]
+        for hop in range(7):
+            ring.append(lax.ppermute(ring[-1], "tp", [(dev, (dev + 1) % 8) for dev in range(8)]))
+        tokens = jnp.roll(
+            jnp.concatenate(ring[::-1], axis=0),
+            (lax.axis_index("tp") + 1) * ring[0].shape[0],
+            axis=0,
+        )
         scales = weights[:, chunk * rows : (chunk + 1) * rows].reshape(tokens.shape[0], -1)
         gate_part = jnp.einsum(
             "nd,edf->enf", tokens, gate_weight, preferred_element_type=jnp.float32

time: 336 us -> 432 us (1.29)
  waiting for transfers between devices: 140 us -> 217 us
  local copies, waits for them, and re-layouts: 5.31 us -> 25.6 us
  blocking collectives: 113 us -> 106 us
    ppermute x0 -> x14, waiting for transfers between devices: none -> 206 us  [body(): lax.ppermute(ring[-1], 'tp', [(dev, (dev + 1) % 8) for dev in range(8)])]
    all_gather x2 -> x0, waiting for transfers between devices: 78 us -> none  [body(): tokens = lax.all_gather(arrived_list[chunk], 'tp', axis=0, tiled=True)]
    reduce_scatter x2, waiting for transfers between devices: 55.6 us -> 2.05 us  [body(): lax.psum_scatter(partial.astype(jnp.bfloat16), 'tp', scatter_dimension=0,...]
    unnamed x16 -> x66, local copies, waits for them, and re-layouts: 0.97 us -> 21.3 us
    all_to_all x1 -> x0, blocking collectives: 7.04 us -> none  [body(): lax.all_to_all(slot_weight, 'ep', split_axis=0, concat_axis=0, tiled=True)]
  transfers between devices with their start and end apart: 7 -> 20, of which waited for: 5 -> 17; matrix products, arithmetic and copies ran while one was open for 16% -> 15% of each run, Pallas kernels for 0% -> 0%
where the time goes in v1:
time: 432 us; the launch traced here: 431 us
  waiting for transfers between devices  217 us (50%)
  blocking collectives  106 us (25%)
  matrix products  52.6 us (12%)
  local copies, waits for them, and re-layouts  25.6 us (6%)
  between operations  14.2 us (3%)
  starting transfers between devices  10.2 us (2%)
  other arithmetic  5.12 us (1%)
    ppermute x14, waiting for transfers between devices, body(): lax.ppermute(ring[-1], 'tp', [(dev, (dev + 1) % 8) for dev in range(8)])  206 us
    all_to_all x2, blocking collectives, body(): lax.all_to_all(outgoing, 'ep', split_axis=0, concat_axis=0, tiled=True)  30.9 us
    dot_general x2, matrix products, body(): jnp.einsum('enf,edf->nd', hidden, down_weight, preferred_element_type=jnp...  26.7 us
    unnamed x66, local copies, waits for them, and re-layouts  21.3 us
    all_gather x2, blocking collectives, body(): lax.all_gather(regrouped[:, section], 'ep', axis=0, tiled=True)  20.5 us
    all_to_all x1, blocking collectives, body(): lax.all_to_all(pooled, 'tp', split_axis=0, concat_axis=1, tiled=True)  17.3 us
    dot_general x2, matrix products, body(): jnp.einsum('nd,edf->enf', tokens, gate_weight, preferred_element_type=jnp...  15.9 us
    all_gather x1, blocking collectives, body(): weights = lax.all_gather(weights, 'tp', axis=0, tiled=True)  14.2 us
  transfers between devices with their start and end apart: 20, of which 17 were waited for; matrix products, arithmetic and copies ran while one was open for 15% of the time, Pallas kernels for 0%

profile of v1, /device:TPU:0, one launch (start us, length us, event | category | flops | bytes accessed | tf_op | source)
XLA Modules:
  0.0 431.4 jit_solution(14777241009007003909)
XLA Ops:
  8.1 1.2 reduce-window.6
  9.8 1.5 fusion.12
  11.3 1.7 convolution_convert_fusion
  13.0 16.3 %all_to_all.85 = bf16[4,48,2048]{2,1,0:T(8,128)(2,1)S(1)} all-to-all(bf16[4,48,2048]{2,1,0:T(8,128)(2,1)S(1)} %bitcast.108), channel_id=1, replica_groups=mesh['ep'=4,'tp'=8] {'ep'}, dimensions={0} | all-to-all | bytes 1572864 | tf_op jit(solution)/shard_map/all_to_all | solution.py:109
  29.4 13.2 %collective-permute-done.8 = bf16[192,2048]{1,0:T(8,128)(2,1)S(1)} collective-permute-done((bf16[192,2048]{1,0:T(8,128)(2,1)S(1)}, bf16[192,2048]{1,0:T(8,128)(2,1)S(1)}, u32[]{:S(2)}, u32[]{:S(2)}) %collective-permute-start.8) | collective-permute-done | bytes 786464 | tf_op jit(solution)/shard_map/ppermute | solution.py:117
  43.5 13.2 %collective-permute-done.9 = bf16[192,2048]{1,0:T(8,128)(2,1)S(1)} collective-permute-done((bf16[192,2048]{1,0:T(8,128)(2,1)S(1)}, bf16[192,2048]{1,0:T(8,128)(2,1)S(1)}, u32[]{:S(2)}, u32[]{:S(2)}) %collective-permute-start.9) | collective-permute-done | bytes 786464 | tf_op jit(solution)/shard_map/ppermute | solution.py:117
  57.6 13.2 %collective-permute-done.10 = bf16[192,2048]{1,0:T(8,128)(2,1)S(1)} collective-permute-done((bf16[192,2048]{1,0:T(8,128)(2,1)S(1)}, bf16[192,2048]{1,0:T(8,128)(2,1)S(1)}, u32[]{:S(2)}, u32[]{:S(2)}) %collective-permute-start.10) | collective-permute-done | bytes 786464 | tf_op jit(solution)/shard_map/ppermute | solution.py:117
  71.7 13.2 %collective-permute-done.11 = bf16[192,2048]{1,0:T(8,128)(2,1)S(1)} collective-permute-done((bf16[192,2048]{1,0:T(8,128)(2,1)S(1)}, bf16[192,2048]{1,0:T(8,128)(2,1)S(1)}, u32[]{:S(2)}, u32[]{:S(2)}) %collective-permute-start.11) | collective-permute-done | bytes 786464 | tf_op jit(solution)/shard_map/ppermute | solution.py:117
  85.8 13.2 %collective-permute-done.12 = bf16[192,2048]{1,0:T(8,128)(2,1)S(1)} collective-permute-done((bf16[192,2048]{1,0:T(8,128)(2,1)S(1)}, bf16[192,2048]{1,0:T(8,128)(2,1)S(1)}, u32[]{:S(2)}, u32[]{:S(2)}) %collective-permute-start.12) | collective-permute-done | bytes 786464 | tf_op jit(solution)/shard_map/ppermute | solution.py:117
  99.9 13.3 %collective-permute-done.13 = bf16[192,2048]{1,0:T(8,128)(2,1)} collective-permute-done((bf16[192,2048]{1,0:T(8,128)(2,1)S(1)}, bf16[192,2048]{1,0:T(8,128)(2,1)}, u32[]{:S(2)}, u32[]{:S(2)}) %collective-permute-start.13) | collective-permute-done | bytes 786464 | tf_op jit(solution)/shard_map/ppermute | solution.py:117
  114.8 3.2 all-to-all-start.3
  118.1 1.6 constant_dynamic-slice_fusion
  119.8 2.9 all-to-all-done.3
  122.7 14.2 %all_gather.15 = f32[32,96,4]{1,2,0:T(4,128)S(1)} all-gather(f32[4,96,4]{1,2,0:T(4,128)S(1)} %all-to-all-done.3), channel_id=1, replica_groups=mesh['ep'=4,'tp'=8] {'tp'}, dimensions={0}, use_global_device_ids=true | all-gather | bytes 55296 | tf_op jit(solution)/shard_map/all_gather | solution.py:112
  137.1 1.3 constant_dynamic-update-slice_fusion.15
  138.5 1.4 constant_dynamic-update-slice_fusion.14
  139.9 1.2 constant_dynamic-update-slice_fusion.13
  141.1 1.2 constant_dynamic-update-slice_fusion.12
  142.6 7.9 %convolution_bitcast_fusion.1 = f32[4,1536,128]{2,1,0:T(8,128)} fusion(bf16[4,2048,128]{2,1,0:T(8,128)(2,1)S(1)} %copy-done.23, s32[]{:T(128)S(6)} %select_n.106, bf16[1536,2048]{1,0:T(8,128)(2,1)S(1)} %constant_dynamic-update-slice_fusion.8), kind=kOutput, calls=%fused_computation.13 | convolution fusion | flops 3233808384 | bytes 11534340 | tf_op jit(solution)/shard_map/nd,edf->enf/dot_general | solution.py:124
  150.5 13.4 %bitcast_convert_fusion = bf16[1536,2048]{1,0:T(8,128)(2,1)} fusion(bf16[4,2048,128]{2,1,0:T(8,128)(2,1)S(1)} %copy-done, bf16[4,2048,128]{2,1,0:T(8,128)(2,1)} %param.20, f32[4,1536,128]{2,1,0:T(8,128)} %convolution_bitcast_fusion.1, s32[]{:T(128)S(6)} %select_n.106, bf16[1536,2048]{1,0:T(8,128)(2,1)} %copy-done.20, f32[4,1536]{1,0:T(4,128)S(1)} %bitcast.113), kind=kOutput, calls=%fused_computation.4 | convolution fusion | flops 6463684608 | bytes 19947524 | tf_op jit(solution)/shard_map/enf,edf->nd/dot_general | solution.py:129
  163.9 1.1 copy-done.1
  165.6 14.5 %all_to_all.86 = bf16[4,48,2048]{2,1,0:T(8,128)(2,1)S(1)} all-to-all(bf16[4,48,2048]{2,1,0:T(8,128)(2,1)S(1)} %bitcast.107), channel_id=1, replica_groups=mesh['ep'=4,'tp'=8] {'ep'}, dimensions={0} | all-to-all | bytes 1572864 | tf_op jit(solution)/shard_map/all_to_all | solution.py:109
  180.1 30.2 %collective-permute-done.1 = bf16[192,2048]{1,0:T(8,128)(2,1)S(1)} collective-permute-done((bf16[192,2048]{1,0:T(8,128)(2,1)S(1)}, bf16[192,2048]{1,0:T(8,128)(2,1)S(1)}, u32[]{:S(2)}, u32[]{:S(2)}) %collective-permute-start.1) | collective-permute-done | bytes 786464 | tf_op jit(solution)/shard_map/ppermute | solution.py:117
  211.2 30.2 %collective-permute-done.2 = bf16[192,2048]{1,0:T(8,128)(2,1)S(1)} collective-permute-done((bf16[192,2048]{1,0:T(8,128)(2,1)S(1)}, bf16[192,2048]{1,0:T(8,128)(2,1)S(1)}, u32[]{:S(2)}, u32[]{:S(2)}) %collective-permute-start.2) | collective-permute-done | bytes 786464 | tf_op jit(solution)/shard_map/ppermute | solution.py:117
  242.3 13.2 %collective-permute-done.3 = bf16[192,2048]{1,0:T(8,128)(2,1)S(1)} collective-permute-done((bf16[192,2048]{1,0:T(8,128)(2,1)S(1)}, bf16[192,2048]{1,0:T(8,128)(2,1)S(1)}, u32[]{:S(2)}, u32[]{:S(2)}) %collective-permute-start.3) | collective-permute-done | bytes 786464 | tf_op jit(solution)/shard_map/ppermute | solution.py:117
  256.4 13.2 %collective-permute-done.4 = bf16[192,2048]{1,0:T(8,128)(2,1)S(1)} collective-permute-done((bf16[192,2048]{1,0:T(8,128)(2,1)S(1)}, bf16[192,2048]{1,0:T(8,128)(2,1)S(1)}, u32[]{:S(2)}, u32[]{:S(2)}) %collective-permute-start.4) | collective-permute-done | bytes 786464 | tf_op jit(solution)/shard_map/ppermute | solution.py:117
  270.5 13.2 %collective-permute-done.5 = bf16[192,2048]{1,0:T(8,128)(2,1)S(1)} collective-permute-done((bf16[192,2048]{1,0:T(8,128)(2,1)S(1)}, bf16[192,2048]{1,0:T(8,128)(2,1)S(1)}, u32[]{:S(2)}, u32[]{:S(2)}) %collective-permute-start.5) | collective-permute-done | bytes 786464 | tf_op jit(solution)/shard_map/ppermute | solution.py:117
  284.6 13.3 %collective-permute-done.6 = bf16[192,2048]{1,0:T(8,128)(2,1)} collective-permute-done((bf16[192,2048]{1,0:T(8,128)(2,1)S(1)}, bf16[192,2048]{1,0:T(8,128)(2,1)}, u32[]{:S(2)}, u32[]{:S(2)}) %collective-permute-start.6) | collective-permute-done | bytes 786464 | tf_op jit(solution)/shard_map/ppermute | solution.py:117
  298.1 13.4 %collective-permute-done.7 = bf16[192,2048]{1,0:T(8,128)(2,1)} collective-permute-done((bf16[192,2048]{1,0:T(8,128)(2,1)}, bf16[192,2048]{1,0:T(8,128)(2,1)}, u32[]{:S(2)}, u32[]{:S(2)}) %collective-permute-start.7) | collective-permute-done | bytes 786464 | tf_op jit(solution)/shard_map/ppermute | solution.py:117
  311.5 1.2 constant_dynamic-update-slice_fusion.7
  312.7 1.2 constant_dynamic-update-slice_fusion.6
  313.8 1.2 constant_dynamic-update-slice_fusion.5
  315.0 1.2 constant_dynamic-update-slice_fusion.4
  316.5 8.0 %convolution_bitcast_fusion.3 = f32[4,1536,128]{2,1,0:T(8,128)} fusion(bf16[4,2048,128]{2,1,0:T(8,128)(2,1)S(1)} %copy-done.24, s32[]{:T(128)S(6)} %select_n.106, bf16[1536,2048]{1,0:T(8,128)(2,1)S(1)} %constant_dynamic-update-slice_fusion), kind=kOutput, calls=%fused_computation.17 | convolution fusion | flops 3233808384 | bytes 11534340 | tf_op jit(solution)/shard_map/nd,edf->enf/dot_general | solution.py:124
  324.5 13.3 %bitcast_convert_fusion.1 = bf16[1536,2048]{1,0:T(8,128)(2,1)} fusion(bf16[4,2048,128]{2,1,0:T(8,128)(2,1)S(1)} %copy-done, bf16[4,2048,128]{2,1,0:T(8,128)(2,1)} %param.20, f32[4,1536,128]{2,1,0:T(8,128)} %convolution_bitcast_fusion.3, s32[]{:T(128)S(6)} %select_n.106, bf16[1536,2048]{1,0:T(8,128)(2,1)} %copy-done.21, f32[4,1536]{1,0:T(4,128)S(1)} %bitcast.112), kind=kOutput, calls=%fused_computation.5 | convolution fusion | flops 6463684608 | bytes 19947524 | tf_op jit(solution)/shard_map/enf,edf->nd/dot_general | solution.py:129
  338.8 3.2 collective-permute-start
  342.1 1.0 collective-permute-done
  343.6 17.3 %all_to_all.87 = bf16[8,128,128]{2,1,0:T(8,128)(2,1)} all-to-all(bf16[8,128,128]{2,1,0:T(8,128)(2,1)S(1)} %bitcast.102), channel_id=1, replica_groups=mesh['ep'=4,'tp'=8] {'tp'}, dimensions={0} | all-to-all | bytes 524288 | tf_op jit(solution)/shard_map/all_to_all | solution.py:141
  361.0 1.1 copy.44
  362.1 11.7 %all_gather.12 = bf16[512,512]{0,1:T(8,128)(2,1)S(1)} all-gather(bf16[128,512]{0,1:T(8,128)(2,1)S(1)} %get-tuple-element.8), channel_id=1, replica_groups=mesh['ep'=4,'tp'=8] {'ep'}, dimensions={0}, use_global_device_ids=true | all-gather | bytes 655360 | tf_op jit(solution)/shard_map/all_gather | solution.py:146
  373.8 8.8 %all_gather.14 = bf16[512,512]{0,1:T(8,128)(2,1)S(1)} all-gather(bf16[128,512]{0,1:T(8,128)(2,1)S(1)} %get-tuple-element.7), channel_id=1, replica_groups=mesh['ep'=4,'tp'=8] {'ep'}, dimensions={0}, use_global_device_ids=true | all-gather | bytes 655360 | tf_op jit(solution)/shard_map/all_gather | solution.py:146
  383.6 10.7 %all_to_all.88 = bf16[4,128,512]{2,1,0:T(8,128)(2,1)S(1)} all-to-all(bf16[4,128,512]{2,1,0:T(8,128)(2,1)S(1)} %bitcast.100), channel_id=1, replica_groups=mesh['ep'=4,'tp'=8] {'ep'}, dimensions={0} | all-to-all | bytes 1048576 | tf_op jit(solution)/shard_map/all_to_all | solution.py:150
  394.2 12.8 %all_to_all.89 = bf16[4,48,2048]{2,1,0:T(8,128)(2,1)} all-to-all(bf16[4,48,2048]{2,1,0:T(8,128)(2,1)} %bitcast.105), channel_id=1, replica_groups=mesh['ep'=4,'tp'=8] {'ep'}, dimensions={0} | all-to-all | bytes 1572864 | tf_op jit(solution)/shard_map/all_to_all | solution.py:133
  407.0 2.0 reduce-scatter.3.cloned.1.call-done
  409.1 3.6 all-to-all-start.4
  413.6 3.0 convolution_bitcast_fusion.4
  416.6 5.3 %all-to-all-done.4 = bf16[4,48,2048]{2,1,0:T(8,128)(2,1)S(1)} async-done(((bf16[4,48,2048]{2,1,0:T(8,128)(2,1)}), bf16[4,48,2048]{2,1,0:T(8,128)(2,1)S(1)}, u32[]{:S(2)}, u32[]{:S(2)}) %all-to-all-start.4) | async-done | bytes 786464 | tf_op jit(solution)/shard_map/all_to_all | solution.py:133
  421.8 3.1 fusion.11
  (119 shorter events, 16.8 us)
Async XLA Ops:
  7.2 143.3 %copy-start = (bf16[4,2048,128]{2,1,0:T(8,128)(2,1)S(1)}, bf16[4,2048,128]{2,1,0:T(8,128)(2,1)}, u32[]{:S(2)}) copy-start(bf16[4,2048,128]{2,1,0:T(8,128)(2,1)} %param.21) | copy-start | bytes 6291460
  29.3 13.2 %collective-permute-start.8 = (bf16[192,2048]{1,0:T(8,128)(2,1)S(1)}, bf16[192,2048]{1,0:T(8,128)(2,1)S(1)}, u32[]{:S(2)}, u32[]{:S(2)}) collective-permute-start(bf16[192,2048]{1,0:T(8,128)(2,1)S(1)} %bitcast.96), channel_id=1, source_target_pairs={{0,1},{1,2},{2,3},{3,4},{4,5},{5,6},{6,7},{7,0},{8,9},{9,10},{10,1... | collective-permute-start | bytes 2359304 | tf_op jit(solution)/shard_map/ppermute | solution.py:117
  42.6 0.9 copy-start.3
  43.5 13.2 %collective-permute-start.9 = (bf16[192,2048]{1,0:T(8,128)(2,1)S(1)}, bf16[192,2048]{1,0:T(8,128)(2,1)S(1)}, u32[]{:S(2)}, u32[]{:S(2)}) collective-permute-start(bf16[192,2048]{1,0:T(8,128)(2,1)S(1)} %collective-permute-done.8), channel_id=1, source_target_pairs={{0,1},{1,2},{2,3},{3,4},{4,5},{5,6},{6,7},{7,0},{8,9},{9,10},{10,1... | collective-permute-start | bytes 2359304 | tf_op jit(solution)/shard_map/ppermute | solution.py:117
  56.7 0.9 copy-start.5
  57.6 13.2 %collective-permute-start.10 = (bf16[192,2048]{1,0:T(8,128)(2,1)S(1)}, bf16[192,2048]{1,0:T(8,128)(2,1)S(1)}, u32[]{:S(2)}, u32[]{:S(2)}) collective-permute-start(bf16[192,2048]{1,0:T(8,128)(2,1)S(1)} %collective-permute-done.9), channel_id=1, source_target_pairs={{0,1},{1,2},{2,3},{3,4},{4,5},{5,6},{6,7},{7,0},{8,9},{9,10},{10,1... | collective-permute-start | bytes 2359304 | tf_op jit(solution)/shard_map/ppermute | solution.py:117
  70.8 0.9 copy-start.7
  71.7 13.2 %collective-permute-start.11 = (bf16[192,2048]{1,0:T(8,128)(2,1)S(1)}, bf16[192,2048]{1,0:T(8,128)(2,1)S(1)}, u32[]{:S(2)}, u32[]{:S(2)}) collective-permute-start(bf16[192,2048]{1,0:T(8,128)(2,1)S(1)} %collective-permute-done.10), channel_id=1, source_target_pairs={{0,1},{1,2},{2,3},{3,4},{4,5},{5,6},{6,7},{7,0},{8,9},{9,10},{10,1... | collective-permute-start | bytes 2359304 | tf_op jit(solution)/shard_map/ppermute | solution.py:117
  84.9 0.9 copy-start.9
  85.8 13.2 %collective-permute-start.12 = (bf16[192,2048]{1,0:T(8,128)(2,1)S(1)}, bf16[192,2048]{1,0:T(8,128)(2,1)S(1)}, u32[]{:S(2)}, u32[]{:S(2)}) collective-permute-start(bf16[192,2048]{1,0:T(8,128)(2,1)S(1)} %collective-permute-done.11), channel_id=1, source_target_pairs={{0,1},{1,2},{2,3},{3,4},{4,5},{5,6},{6,7},{7,0},{8,9},{9,10},{10,1... | collective-permute-start | bytes 2359304 | tf_op jit(solution)/shard_map/ppermute | solution.py:117
  99.0 0.9 copy-start.10
  99.9 13.3 %collective-permute-start.13 = (bf16[192,2048]{1,0:T(8,128)(2,1)S(1)}, bf16[192,2048]{1,0:T(8,128)(2,1)}, u32[]{:S(2)}, u32[]{:S(2)}) collective-permute-start(bf16[192,2048]{1,0:T(8,128)(2,1)S(1)} %collective-permute-done.12), channel_id=1, source_target_pairs={{0,1},{1,2},{2,3},{3,4},{4,5},{5,6},{6,7},{7,0},{8,9},{9,10},{10,1... | collective-permute-start | bytes 2359304 | tf_op jit(solution)/shard_map/ppermute | solution.py:117
  113.2 23.9 %collective-permute-start.14 = (bf16[192,2048]{1,0:T(8,128)(2,1)}, bf16[192,2048]{1,0:T(8,128)(2,1)}, u32[]{:S(2)}, u32[]{:S(2)}) collective-permute-start(bf16[192,2048]{1,0:T(8,128)(2,1)} %collective-permute-done.13), channel_id=1, source_target_pairs={{0,1},{1,2},{2,3},{3,4},{4,5},{5,6},{6,7},{7,0},{8,9},{9,10},{10,1... | collective-permute-start | bytes 2359304 | tf_op jit(solution)/shard_map/ppermute | solution.py:117
  114.8 7.9 %all-to-all-start.3 = ((f32[4,96,4]{1,2,0:T(4,128)}), f32[4,96,4]{1,2,0:T(4,128)S(1)}, u32[]{:S(2)}, u32[]{:S(2)}) async-start(f32[4,96,4]{1,2,0:T(4,128)} %fusion.41), calls=%async_computation.3 | async-start | bytes 16384 | tf_op jit(solution)/shard_map/all_to_all | solution.py:111
  118.1 62.1 %all-gather.2.cloned.1.call-start = ((), (), s32[]{:S(2)}) async-start(), calls=%async_computation.9 | async-start | bytes 1179648 | tf_op jit(solution)/shard_map/all_gather | solution.py:95
  119.7 274.5 %reduce-scatter.5.cloned.1.call-start = ((), (), s32[]{:S(2)}) async-start(), calls=%async_computation.11 | async-start | bytes 7077888 | tf_op jit(solution)/shard_map/reduce_scatter | solution.py:130
  137.1 5.2 %copy-start.8 = (bf16[192,2048]{1,0:T(8,128)(2,1)S(1)}, bf16[192,2048]{1,0:T(8,128)(2,1)}, u32[]{:S(2)}) copy-start(bf16[192,2048]{1,0:T(8,128)(2,1)} %copy-done.7) | copy-start | bytes 2359300
  137.1 5.2 %copy-start.6 = (bf16[192,2048]{1,0:T(8,128)(2,1)S(1)}, bf16[192,2048]{1,0:T(8,128)(2,1)}, u32[]{:S(2)}) copy-start(bf16[192,2048]{1,0:T(8,128)(2,1)} %copy-done.5) | copy-start | bytes 2359300
  137.1 5.3 %copy-start.4 = (bf16[192,2048]{1,0:T(8,128)(2,1)S(1)}, bf16[192,2048]{1,0:T(8,128)(2,1)}, u32[]{:S(2)}) copy-start(bf16[192,2048]{1,0:T(8,128)(2,1)} %copy-done.3) | copy-start | bytes 2359300
  137.1 5.4 %copy-start.23 = (bf16[4,2048,128]{2,1,0:T(8,128)(2,1)S(1)}, bf16[4,2048,128]{2,1,0:T(8,128)(2,1)}, u32[]{:S(2)}) copy-start(bf16[4,2048,128]{2,1,0:T(8,128)(2,1)} %param.19) | copy-start | bytes 6291460
  142.5 7.9 %copy-start.20 = (bf16[1536,2048]{1,0:T(8,128)(2,1)}, bf16[1536,2048]{1,0:T(8,128)(2,1)S(1)}, u32[]{:S(2)}) copy-start(bf16[1536,2048]{1,0:T(8,128)(2,1)S(1)} %constant_dynamic-update-slice_fusion.8) | copy-start | bytes 18874372
  163.8 1.2 copy-start.1
  163.8 1.2 copy-start.25
  163.9 245.2 %reduce-scatter.3.cloned.1.call-start = ((), (), s32[]{:S(2)}) async-start(), calls=%async_computation.10 | async-start | bytes 7077888 | tf_op jit(solution)/shard_map/reduce_scatter | solution.py:130
  180.1 30.2 %collective-permute-start.1 = (bf16[192,2048]{1,0:T(8,128)(2,1)S(1)}, bf16[192,2048]{1,0:T(8,128)(2,1)S(1)}, u32[]{:S(2)}, u32[]{:S(2)}) collective-permute-start(bf16[192,2048]{1,0:T(8,128)(2,1)S(1)} %bitcast.98), channel_id=1, source_target_pairs={{0,1},{1,2},{2,3},{3,4},{4,5},{5,6},{6,7},{7,0},{8,9},{9,10},{10,1... | collective-permute-start | bytes 2359304 | tf_op jit(solution)/shard_map/ppermute | solution.py:117
  210.3 0.9 copy-start.11
  211.2 30.2 %collective-permute-start.2 = (bf16[192,2048]{1,0:T(8,128)(2,1)S(1)}, bf16[192,2048]{1,0:T(8,128)(2,1)S(1)}, u32[]{:S(2)}, u32[]{:S(2)}) collective-permute-start(bf16[192,2048]{1,0:T(8,128)(2,1)S(1)} %collective-permute-done.1), channel_id=1, source_target_pairs={{0,1},{1,2},{2,3},{3,4},{4,5},{5,6},{6,7},{7,0},{8,9},{9,10},{10,1... | collective-permute-start | bytes 2359304 | tf_op jit(solution)/shard_map/ppermute | solution.py:117
  241.4 0.9 copy-start.13
  242.3 13.2 %collective-permute-start.3 = (bf16[192,2048]{1,0:T(8,128)(2,1)S(1)}, bf16[192,2048]{1,0:T(8,128)(2,1)S(1)}, u32[]{:S(2)}, u32[]{:S(2)}) collective-permute-start(bf16[192,2048]{1,0:T(8,128)(2,1)S(1)} %collective-permute-done.2), channel_id=1, source_target_pairs={{0,1},{1,2},{2,3},{3,4},{4,5},{5,6},{6,7},{7,0},{8,9},{9,10},{10,1... | collective-permute-start | bytes 2359304 | tf_op jit(solution)/shard_map/ppermute | solution.py:117
  255.5 0.9 copy-start.15
  256.4 13.2 %collective-permute-start.4 = (bf16[192,2048]{1,0:T(8,128)(2,1)S(1)}, bf16[192,2048]{1,0:T(8,128)(2,1)S(1)}, u32[]{:S(2)}, u32[]{:S(2)}) collective-permute-start(bf16[192,2048]{1,0:T(8,128)(2,1)S(1)} %collective-permute-done.3), channel_id=1, source_target_pairs={{0,1},{1,2},{2,3},{3,4},{4,5},{5,6},{6,7},{7,0},{8,9},{9,10},{10,1... | collective-permute-start | bytes 2359304 | tf_op jit(solution)/shard_map/ppermute | solution.py:117
  269.7 0.9 copy-start.17
  270.5 13.2 %collective-permute-start.5 = (bf16[192,2048]{1,0:T(8,128)(2,1)S(1)}, bf16[192,2048]{1,0:T(8,128)(2,1)S(1)}, u32[]{:S(2)}, u32[]{:S(2)}) collective-permute-start(bf16[192,2048]{1,0:T(8,128)(2,1)S(1)} %collective-permute-done.4), channel_id=1, source_target_pairs={{0,1},{1,2},{2,3},{3,4},{4,5},{5,6},{6,7},{7,0},{8,9},{9,10},{10,1... | collective-permute-start | bytes 2359304 | tf_op jit(solution)/shard_map/ppermute | solution.py:117
  283.7 0.9 copy-start.18
  284.6 13.3 %collective-permute-start.6 = (bf16[192,2048]{1,0:T(8,128)(2,1)S(1)}, bf16[192,2048]{1,0:T(8,128)(2,1)}, u32[]{:S(2)}, u32[]{:S(2)}) collective-permute-start(bf16[192,2048]{1,0:T(8,128)(2,1)S(1)} %collective-permute-done.5), channel_id=1, source_target_pairs={{0,1},{1,2},{2,3},{3,4},{4,5},{5,6},{6,7},{7,0},{8,9},{9,10},{10,1... | collective-permute-start | bytes 2359304 | tf_op jit(solution)/shard_map/ppermute | solution.py:117
  297.9 13.5 %collective-permute-start.7 = (bf16[192,2048]{1,0:T(8,128)(2,1)}, bf16[192,2048]{1,0:T(8,128)(2,1)}, u32[]{:S(2)}, u32[]{:S(2)}) collective-permute-start(bf16[192,2048]{1,0:T(8,128)(2,1)} %collective-permute-done.6), channel_id=1, source_target_pairs={{0,1},{1,2},{2,3},{3,4},{4,5},{5,6},{6,7},{7,0},{8,9},{9,10},{10,1... | collective-permute-start | bytes 2359304 | tf_op jit(solution)/shard_map/ppermute | solution.py:117
  298.1 18.2 %copy-start.16 = (bf16[192,2048]{1,0:T(8,128)(2,1)S(1)}, bf16[192,2048]{1,0:T(8,128)(2,1)}, u32[]{:S(2)}) copy-start(bf16[192,2048]{1,0:T(8,128)(2,1)} %copy-done.15) | copy-start | bytes 2359300
  298.1 18.2 %copy-start.14 = (bf16[192,2048]{1,0:T(8,128)(2,1)S(1)}, bf16[192,2048]{1,0:T(8,128)(2,1)}, u32[]{:S(2)}) copy-start(bf16[192,2048]{1,0:T(8,128)(2,1)} %copy-done.13) | copy-start | bytes 2359300
  298.1 18.3 %copy-start.12 = (bf16[192,2048]{1,0:T(8,128)(2,1)S(1)}, bf16[192,2048]{1,0:T(8,128)(2,1)}, u32[]{:S(2)}) copy-start(bf16[192,2048]{1,0:T(8,128)(2,1)} %copy-done.11) | copy-start | bytes 2359300
  298.1 18.4 %copy-start.24 = (bf16[4,2048,128]{2,1,0:T(8,128)(2,1)S(1)}, bf16[4,2048,128]{2,1,0:T(8,128)(2,1)}, u32[]{:S(2)}) copy-start(bf16[4,2048,128]{2,1,0:T(8,128)(2,1)} %param.19) | copy-start | bytes 6291460
  316.5 8.0 %copy-start.21 = (bf16[1536,2048]{1,0:T(8,128)(2,1)}, bf16[1536,2048]{1,0:T(8,128)(2,1)S(1)}, u32[]{:S(2)}) copy-start(bf16[1536,2048]{1,0:T(8,128)(2,1)S(1)} %constant_dynamic-update-slice_fusion) | copy-start | bytes 18874372
  337.8 0.9 copy-start.19
  337.8 5.5 %copy-start.22 = (f32[128]{0:T(128)S(1)}, f32[128]{0:T(128)}, u32[]{:S(2)}) copy-start(f32[128]{0:T(128)} %param.13) | copy-start | bytes 1540
  338.8 43.9 %copy-start.2 = (bf16[1024,512]{1,0:T(8,128)(2,1)S(1)}, bf16[1024,512]{1,0:T(8,128)(2,1)}, u32[]{:S(2)}) copy-start(bf16[1024,512]{1,0:T(8,128)(2,1)} %all-gather.2.cloned.1.call-done) | copy-start | bytes 3145732
  338.8 4.2 collective-permute-start
  409.1 12.7 %all-to-all-start.4 = ((bf16[4,48,2048]{2,1,0:T(8,128)(2,1)}), bf16[4,48,2048]{2,1,0:T(8,128)(2,1)S(1)}, u32[]{:S(2)}, u32[]{:S(2)}) async-start(bf16[4,48,2048]{2,1,0:T(8,128)(2,1)} %bitcast.106), calls=%async_computation.5 | async-start | bytes 1572864 | tf_op jit(solution)/shard_map/all_to_all | solution.py:133
Sparse Core Ops, SparseCore 0:
  121.0 23.5 all-gather.1
  164.0 83.0 reduce-scatter.4
  338.0 71.0 reduce-scatter.2
